TPU v7x, 32 devices: a whole 2x2x4 slice. The times are simulated.
32 devices in a mesh: sp: 8 (over z, y), fs: 2 (over x), tp: 2 (over core).
Axes of the slice: x: 2, y: 2, z: 4, core: 2. Of those that a mesh axis runs over, the one named last changes fastest.
Arguments:
- tokens: bfloat16 [8192, 2048], P(('fs', 'sp', 'tp')), parts along dimension 0, may hold values from -60 to 60
- norm_gain: float32 [2048], replicated, may hold values from 0.1 to 1.9
- pool_in: bfloat16 [2048, 512], P('sp', 'tp'), may hold values from -0.125 to 0.125
- gate_in: bfloat16 [2048, 1024], P('sp', 'tp'), may hold values from -0.125 to 0.125
- value_in: bfloat16 [2048, 1024], P('sp', 'tp'), may hold values from -0.125 to 0.125
- pool_mix: bfloat16 [4, 128, 128], P('tp'), may hold values from -0.5 to 0.5
- averaging_factor: float32 [512], P('tp'), may hold values from 0.25 to 0.75
- conv_taps: float32 [4, 1024], P(None, 'tp'), may hold values from -3 to 3
- rate_mix: bfloat16 [16, 64, 64], P('tp'), may hold values from -0.75 to 0.75
- input_mix: bfloat16 [16, 64, 64], P('tp'), may hold values from -0.75 to 0.75
- log_rate: float32 [1024], P('tp'), may hold values from 1.5 to 16
- decay_shift: float32 [32, 4096], P(('fs', 'tp'), 'sp'), parts along dimension 0, may hold values from -1.1 to 0
- initial_state: float32 [2048], P(('fs', 'tp')), parts along dimension 0, may hold values from -6 to 6
- out_pool: bfloat16 [2048, 512], P('sp', 'tp'), may hold values from -0.15625 to 0.15625
- out_rnn: bfloat16 [2048, 1024], P('sp', 'tp'), may hold values from -0.15625 to 0.15625
Outputs:
- mixed: bfloat16 [8192, 2048], P(('fs', 'sp', 'tp')), parts along dimension 0
There are 2 independent parts, one for each index of `fs`. A program takes and returns all parts, laid end to end along the dimension named above; an argument that names none is the same for every part. Nothing has to cross between parts.
All inputs are finite; a program needn't handle non-finite values.
Results may differ from a plain program's by a relative error of at most 0.012.
Values may be sent and summed in bfloat16 or wider, within the bound.
No kernel may reach another device: no remote copies, remote signals or barrier semaphores. Data moves between devices by JAX's collectives and lax.ppermute only.
A program may use at most 64 MiB of HBM per device.

v0:
```python
import jax
import jax.numpy as jnp
from jax import lax
from jax.sharding import PartitionSpec as P

GROUP_WIDTH = 128
HEAD_DIM = 64
TAPS = 4
REACH = 16
epsilon = 1e-06
sharpness = 8.0


def from_behind(value, axis, steps):
    count = lax.axis_size(axis)
    first, last = (max(0, -steps), min(count, count - steps))
    return lax.ppermute(value, axis, [(source, source + steps) for source in range(first, last)])


def carried_in(array, axis, combine, identity):
    count, index = (lax.axis_size(axis), lax.axis_index(axis))
    everything = jax.tree.map(lambda part: lax.all_gather(part, axis), array)
    start = jax.tree.map(
        lambda part, zero: jnp.broadcast_to(jnp.asarray(zero, part.dtype), part.shape),
        array,
        identity,
    )

    def hop(k, before):
        reached = k < index
        new = combine(before, jax.tree.map(lambda part: part[k], everything))
        return jax.tree.map(lambda a, b: jnp.where(reached, a, b), new, before)

    return lax.fori_loop(0, count, hop, start)


def chain_pairs(first_pair, second_pair):
    return (first_pair[0] * second_pair[0], second_pair[0] * first_pair[1] + second_pair[1])


def right_product(left_rows, weight_rows):
    return lax.dot_general(
        left_rows, weight_rows, (((1,), (1,)), ((), ())), preferred_element_type=jnp.float32
    )


def shards(
    tokens,
    norm_gain,
    pool_in,
    gate_in,
    value_in,
    pool_mix,
    averaging_factor,
    conv_taps,
    rate_mix,
    input_mix,
    log_rate,
    decay_shift,
    initial_state,
    out_pool,
    out_rnn,
):
    tp_index = lax.axis_index("tp")
    sp_index = lax.axis_index("sp")
    gathered = (
        lax.all_gather(pool_in, "sp", axis=0, tiled=True),
        lax.all_gather(gate_in, "sp", axis=0, tiled=True),
        lax.all_gather(value_in, "sp", axis=0, tiled=True),
        lax.all_gather(out_pool, "sp", axis=0, tiled=True),
        lax.all_gather(out_rnn, "sp", axis=0, tiled=True),
    )
    pool_weight, gate_weight, value_weight, averaging_exit_matrix, out_rnn_weight = gathered
    pool_width = pool_weight.shape[1]
    rnn_width = gate_weight.shape[1]
    widened = lax.all_gather(tokens, "tp", axis=0, tiled=True).astype(jnp.float32)
    scaling = lax.rsqrt(jnp.mean(widened * widened, axis=1, keepdims=True) + epsilon)
    normed = (widened * scaling * norm_gain[None, :]).astype(jnp.bfloat16)
    outputs = [
        jnp.dot(normed, matrix, preferred_element_type=jnp.float32).astype(jnp.bfloat16)
        for matrix in (pool_weight, gate_weight, value_weight)
    ]
    projected = jnp.concatenate(outputs, axis=1)
    block_rows = projected.shape[0]
    pool_pre = projected[:, :pool_width]
    gate_pre = projected[:, pool_width : pool_width + rnn_width]
    value_pre = projected[:, pool_width + rnn_width :]
    edge_rows = jnp.concatenate(
        [pool_pre[block_rows - REACH :], value_pre[block_rows - REACH :]], axis=1
    )
    earlier_rows = from_behind(edge_rows, "sp", 1)
    pool_values = pool_pre.astype(jnp.float32)
    pool_padded = jnp.concatenate([earlier_rows[:, :pool_width], pool_pre], axis=0).astype(
        jnp.float32
    )
    value_padded = jnp.concatenate([earlier_rows[:, pool_width:], value_pre], axis=0).astype(
        jnp.float32
    )
    groups_here = pool_width // GROUP_WIDTH
    group_index = tp_index * groups_here + jnp.arange(pool_width, dtype=jnp.int32) // GROUP_WIDTH
    window = jnp.left_shift(jnp.int32(2), group_index)
    positions = sp_index * block_rows + jnp.arange(block_rows, dtype=jnp.int32)
    window_sum = jnp.zeros((block_rows, pool_width), jnp.float32)
    for steps_back in range(REACH):
        lagged = pool_padded[REACH - steps_back : REACH - steps_back + block_rows]
        window_sum = window_sum + jnp.where(steps_back < window[None, :], lagged, 0.0)
    counts = jnp.minimum(positions[:, None] + 1, window[None, :]).astype(jnp.float32)
    pooled = (window_sum / counts - pool_values).astype(jnp.bfloat16)
    grouped = pooled.reshape(block_rows, groups_here, GROUP_WIDTH)
    mixed_groups = jnp.einsum("tgc,gcd->tgd", grouped, pool_mix, preferred_element_type=jnp.float32)
    pool_out = (mixed_groups.reshape(block_rows, pool_width) * averaging_factor[None, :]).astype(
        jnp.bfloat16
    )
    start_row = REACH - TAPS + 1
    convolved = conv_taps[0][None, :] * value_padded[start_row : start_row + block_rows]
    for tap_index in range(1, TAPS):
        convolved = (
            convolved
            + conv_taps[tap_index][None, :]
            * value_padded[start_row + tap_index : start_row + tap_index + block_rows]
        )
    conv_out = convolved.astype(jnp.bfloat16)
    heads_here = rnn_width // HEAD_DIM
    both_mixes = jnp.concatenate([rate_mix, input_mix], axis=2)
    gate_terms = jnp.einsum(
        "thc,hcd->thd",
        conv_out.reshape(block_rows, heads_here, HEAD_DIM),
        both_mixes,
        preferred_element_type=jnp.float32,
    )
    rate_gate = jax.nn.sigmoid(gate_terms[:, :, :HEAD_DIM]).reshape(block_rows, rnn_width)
    input_gate = jax.nn.sigmoid(gate_terms[:, :, HEAD_DIM:]).reshape(block_rows, rnn_width)
    shifts = jnp.broadcast_to(
        jnp.transpose(decay_shift)[:, :, None], (block_rows, heads_here, HEAD_DIM)
    ).reshape(block_rows, rnn_width)
    log_decay = -sharpness * rate_gate * jax.nn.softplus(-log_rate)[None, :] + shifts
    decays = jnp.exp(log_decay)
    drives = jnp.sqrt(-jnp.expm1(2.0 * log_decay)) * input_gate * conv_out.astype(jnp.float32)
    cumulative, local_state = lax.associative_scan(chain_pairs, (decays, drives), axis=0)
    identity = (jnp.ones((rnn_width,), jnp.float32), jnp.zeros((rnn_width,), jnp.float32))
    prior_decay, prior_state = carried_in(
        (cumulative[block_rows - 1], local_state[block_rows - 1]), "sp", chain_pairs, identity
    )
    carried = prior_decay * initial_state + prior_state
    hidden_state = local_state + cumulative * carried[None, :]
    rnn_out = (jax.nn.gelu(gate_pre.astype(jnp.float32), approximate=True) * hidden_state).astype(
        jnp.bfloat16
    )
    return lax.psum_scatter(
        right_product(pool_out, averaging_exit_matrix) + right_product(rnn_out, out_rnn_weight),
        "tp",
        scatter_dimension=0,
        tiled=True,
    ).astype(jnp.bfloat16)


def solution(mesh):
    placed = (
        P(("fs", "sp", "tp"), None),
        P(),
        P("sp", "tp"),
        P("sp", "tp"),
        P("sp", "tp"),
        P("tp", None, None),
        P("tp"),
        P(None, "tp"),
        P("tp", None, None),
        P("tp", None, None),
        P("tp"),
        P(("fs", "tp"), "sp"),
        P(("fs", "tp")),
        P("sp", "tp"),
        P("sp", "tp"),
    )
    return jax.shard_map(
        shards, mesh=mesh, in_specs=placed, out_specs=P(("fs", "sp", "tp"), None), check_vma=False
    )
```

profile of v0, /device:TPU:0, one launch (start us, length us, event | category | flops | bytes accessed | tf_op | source)
XLA Modules:
  0.0 381.2 jit_solution(15395088567445469416)
XLA Ops:
  15.7 6.6 %all-gather.9.cloned.1.call-done = bf16[512,2048]{1,0:T(8,128)(2,1)} async-done(((bf16[256,2048]{1,0:T(8,128)(2,1)}), bf16[512,2048]{1,0:T(8,128)(2,1)}) %all-gather.9.cloned.1.call-update) | async-done | bytes 2097168 | tf_op jit(solution)/shard_map/all_gather | solution.py:76
  22.2 2.2 fusion
  24.5 41.4 %all-gather.11.cloned.1.call-done = bf16[2048,256]{1,0:T(8,128)(2,1)} async-done(((bf16[256,256]{1,0:T(8,128)(2,1)}), bf16[2048,256]{1,0:T(8,128)(2,1)}) %all-gather.11.cloned.1.call-update) | async-done | bytes 1048592 | tf_op jit(solution)/shard_map/all_gather | solution.py:67
  65.8 2.0 convolution_convert_fusion.2
  68.6 47.2 %all-gather.13.cloned.1.call-done = bf16[2048,512]{1,0:T(8,128)(2,1)} async-done(((bf16[256,512]{1,0:T(8,128)(2,1)}), bf16[2048,512]{1,0:T(8,128)(2,1)}) %all-gather.13.cloned.1.call-update) | async-done | bytes 2097168 | tf_op jit(solution)/shard_map/all_gather | solution.py:69
  115.8 2.9 convolution_convert_fusion.1
  119.5 2.6 collective-permute-start
  127.2 2.1 copy.30
  129.2 1.6 convolution_bitcast_fusion
  130.9 1.9 fusion.12
  132.8 2.5 copy.31
  135.3 2.6 copy.33
  137.9 4.4 %convert_multiply_fusion.5 = (f32[512,512]{1,0:T(8,128)}, f32[512,512]{1,0:T(8,128)}) fusion(f32[512,512]{1,0:T(8,128)} %copy.33, f32[512,512]{1,0:T(8,128)} %copy.32, f32[512,512]{1,0:T(8,128)} %copy.31, f32[512]{0:T(512)S(1)} %fusion.63, f32[528,512]{1,0:T(8,128)S(1)} %maximum_convert_fusion, f32[512]{0:T(512)S(1)} %bitcast.61, f32[512]{0:T(512)S(1)} %bitcast.63, ...), kind=kLoop, calls=%fused_computation.41 | loop fusion | flops 3932160 | bytes 9447424 | tf_op jit(solution)/shard_map/mul | solution.py:138
  142.2 3.7 slice.389
  146.0 3.6 slice.390
  149.6 2.1 slice.388
  151.7 2.1 slice.392
  153.7 2.7 multiply_add_fusion.1
  156.5 2.5 slice.395
  158.9 2.5 slice.396
  161.4 2.5 slice.394
  163.9 2.5 slice.398
  166.4 2.0 multiply_add_fusion.2
  171.4 1.6 slice.404
  173.0 1.9 multiply_add_fusion.3
  225.3 1.6 slice.399
  229.7 2.5 slice.393
  232.3 2.5 slice.450
  237.4 2.1 slice.387
  239.5 3.7 slice.452
  249.8 1.9 fusion.49
  253.7 4.6 %pad.127 = f32[512,512]{1,0:T(8,128)} pad(f32[256,512]{1,0:T(8,128)} %add.492, f32[]{:T(128)} %constant.117.clone.1), padding=1_0_1x0_0_0 | pad | bytes 1572868 | tf_op jit(solution)/shard_map/pad | solution.py:139
  258.3 1.7 pad_maximum_fusion.3
  260.0 2.6 pad.142
  262.6 1.6 pad.143
  264.3 2.1 add.502
  266.3 2.7 fusion.20
  269.9 4.6 %pad.126 = f32[512,512]{1,0:T(8,128)} pad(f32[256,512]{1,0:T(8,128)} %pad_maximum_fusion, f32[]{:T(128)} %constant.117.clone.1), padding=0_1_1x0_0_0 | pad | bytes 1572868 | tf_op jit(solution)/shard_map/pad | solution.py:139
  275.2 26.7 %all-gather.1 = f32[8,1,512]{2,1,0:T(1,128)S(1)} all-gather(f32[1,1,512]{2,1,0:T(1,128)S(1)} %add_bitcast_fusion), channel_id=1, replica_groups=mesh['sp'=8,'fs'=2,'tp'=2] {'sp'}, dimensions={0}, use_global_device_ids=true | all-gather | bytes 18432 | tf_op jit(solution)/shard_map/all_gather | solution.py:22
  301.9 4.7 %pad.145 = f32[512,512]{1,0:T(8,128)} pad(f32[256,512]{1,0:T(8,128)} %add.502, f32[]{:T(128)} %constant.117.clone.1), padding=1_0_1x0_0_0 | pad | bytes 1572868 | tf_op jit(solution)/shard_map/pad | solution.py:139
  306.6 1.9 pad_maximum_fusion.1
  308.6 4.6 %pad.144 = f32[512,512]{1,0:T(8,128)} pad(f32[256,512]{1,0:T(8,128)} %pad_maximum_fusion.1, f32[]{:T(128)} %constant.117.clone.1), padding=0_1_1x0_0_0 | pad | bytes 1572868 | tf_op jit(solution)/shard_map/pad | solution.py:139
  313.9 26.3 %all-gather = f32[8,1,512]{2,1,0:T(1,128)S(1)} all-gather(f32[1,1,512]{2,1,0:T(1,128)S(1)} %add_bitcast_fusion.1), channel_id=1, replica_groups=mesh['sp'=8,'fs'=2,'tp'=2] {'sp'}, dimensions={0}, use_global_device_ids=true | all-gather | bytes 18432 | tf_op jit(solution)/shard_map/all_gather | solution.py:22
  341.6 7.2 %fusion.46 = f32[2,512,128]{1,2,0:T(8,128)S(1)} fusion(bf16[2,128,128]{2,1,0:T(8,128)(2,1)S(1)} %copy-done, bf16[512,256]{1,0:T(8,128)(2,1)S(1)} %copy-done.8, s32[256]{0:T(256)S(1)} %copy-done.46, s32[512]{0:T(512)S(1)} %copy-done.42, f32[528,256]{1,0:T(8,128)} %maximum_convert_fusion.1, pred[256]{0:T(512)(128)(4,1)S(1)} %copy-done.47, ...), kind=kOutput, calls=%fused_computation.93 | convolution fusion | flops 38404096 | bytes 9250560 | tf_op jit(solution)/shard_map/tgc,gcd->tgd/dot_general | solution.py:110
  349.0 4.0 %fusion.77 = f32[512,2048]{1,0:T(8,128)} fusion(bf16[512,256]{0,1:T(8,128)(2,1)S(1)} %fusion.38, bf16[2048,256]{1,0:T(8,128)(2,1)} %all-gather.15.cloned.1.call-done), kind=kOutput, calls=%fused_computation.191 | convolution fusion | flops 536870912 | bytes 5505024 | tf_op jit(solution)/shard_map/dot_general | solution.py:42
  353.0 9.1 %convolution_add_fusion = f32[512,2048]{1,0:T(8,128)} fusion(f32[512,2048]{1,0:T(8,128)} %fusion.77, bf16[2048,512]{1,0:T(8,128)(2,1)} %all-gather.19.cloned.1.call-done, bf16[2048,512]{1,0:T(8,128)(2,1)} %all-gather.17.cloned.1.call-done, f32[512,512]{1,0:T(8,128)} %pad.144, f32[512,512]{1,0:T(8,128)} %pad.145, f32[512,512]{1,0:T(8,128)} %pad.126, ...), kind=kOutput, calls=%fused_computation.9 | convolution fusion | flops 2156920832 | bytes 18886656 | tf_op jit(solution)/shard_map/dot_general | solution.py:42
  362.2 9.4 %reduce-scatter.2.cloned.1.call-done = f32[256,2048]{1,0:T(8,128)} async-done(((f32[512,2048]{1,0:T(8,128)}), f32[256,2048]{1,0:T(8,128)}) %reduce-scatter.2.cloned.1.call-update) | async-done | bytes 2097168 | tf_op jit(solution)/shard_map/reduce_scatter | solution.py:149
  371.6 2.7 convert_element_type.63
  (282 shorter events, 86.5 us)
Async XLA Ops:
  6.5 335.0 %copy-start = (bf16[2,128,128]{2,1,0:T(8,128)(2,1)S(1)}, bf16[2,128,128]{2,1,0:T(8,128)(2,1)}, u32[]{:S(2)}) copy-start(bf16[2,128,128]{2,1,0:T(8,128)(2,1)} %param.22) | copy-start | bytes 196612
  6.5 8.5 %copy-start.37 = (f32[4,512]{1,0:T(4,128)S(1)}, f32[4,512]{1,0:T(4,128)}, u32[]{:S(2)}) copy-start(f32[4,512]{1,0:T(4,128)} %param.24) | copy-start | bytes 24580
  6.5 8.5 %copy-start.43 = (f32[512]{0:T(512)S(1)}, f32[512]{0:T(512)}, u32[]{:S(2)}) copy-start(f32[512]{0:T(512)} %param.27) | copy-start | bytes 6148
  6.5 59.3 %copy-start.23 = (f32[2048]{0:T(1024)S(1)}, f32[2048]{0:T(1024)}, u32[]{:S(2)}) copy-start(f32[2048]{0:T(1024)} %param.18) | copy-start | bytes 24580
  6.5 15.7 %all-gather.9.cloned.1.call-start = ((), (), s32[]{:S(2)}) async-start(), calls=%async_computation.1 | async-start | bytes 3145728 | tf_op jit(solution)/shard_map/all_gather | solution.py:76
  7.3 58.6 %all-gather.11.cloned.1.call-start = ((), (), s32[]{:S(2)}) async-start(), calls=%async_computation.2 | async-start | bytes 1179648 | tf_op jit(solution)/shard_map/all_gather | solution.py:67
  8.0 107.8 %all-gather.13.cloned.1.call-start = ((), (), s32[]{:S(2)}) async-start(), calls=%async_computation.3 | async-start | bytes 2359296 | tf_op jit(solution)/shard_map/all_gather | solution.py:69
  8.8 340.3 %all-gather.15.cloned.1.call-start = ((), (), s32[]{:S(2)}) async-start(), calls=%async_computation.4 | async-start | bytes 1179648 | tf_op jit(solution)/shard_map/all_gather | solution.py:70
  9.3 343.7 %all-gather.17.cloned.1.call-start = ((), (), s32[]{:S(2)}) async-start(), calls=%async_computation.5 | async-start | bytes 2359296 | tf_op jit(solution)/shard_map/all_gather | solution.py:68
  9.9 343.1 %all-gather.19.cloned.1.call-start = ((), (), s32[]{:S(2)}) async-start(), calls=%async_computation.6 | async-start | bytes 2359296 | tf_op jit(solution)/shard_map/all_gather | solution.py:71
  10.5 361.1 %reduce-scatter.2.cloned.1.call-start = ((), (), s32[]{:S(2)}) async-start(), calls=%async_computation.7 | async-start | bytes 6291456 | tf_op jit(solution)/shard_map/reduce_scatter | solution.py:149
  22.2 43.6 %copy-start.1 = (bf16[512,2048]{1,0:T(8,128)(2,1)S(1)}, bf16[512,2048]{1,0:T(8,128)(2,1)}, u32[]{:S(2)}) copy-start(bf16[512,2048]{1,0:T(8,128)(2,1)} %all-gather.9.cloned.1.call-done) | copy-start | bytes 6291460
  24.5 91.3 %copy-start.25 = (f32[512]{0:T(512)}, f32[512]{0:T(512)S(1)}, u32[]{:S(2)}) copy-start(f32[512]{0:T(512)S(1)} %add_rsqrt_fusion) | copy-start | bytes 6148
  68.6 54.1 %copy-start.20 = (f32[8,512]{1,0:T(8,128)S(1)}, f32[8,512]{1,0:T(8,128)}, u32[]{:S(2)}) copy-start(f32[8,512]{1,0:T(8,128)} %param.28) | copy-start | bytes 49156
  119.5 4.6 %collective-permute-start = (bf16[16,768]{1,0:T(8,128)(2,1)S(1)}, bf16[16,768]{1,0:T(8,128)(2,1)S(1)}, u32[]{:S(2)}, u32[]{:S(2)}) collective-permute-start(bf16[16,768]{1,0:T(8,128)(2,1)S(1)} %pad_maximum_fusion.10), channel_id=1, source_target_pairs={{0,4},{4,8},{8,12},{12,16},{16,20},{20,24},{24,28},{1,5},{5,9},{9,... | collective-permute-start | bytes 73736 | tf_op jit(solution)/shard_map/ppermute | solution.py:17
  142.2 7.4 %copy-start.2 = (f32[512,512]{1,0:T(8,128)S(1)}, f32[512,512]{1,0:T(8,128)}, u32[]{:S(2)}) copy-start(f32[512,512]{1,0:T(8,128)} %get-tuple-element.155) | copy-start | bytes 3145732
  229.6 15.5 %copy-start.38 = (f32[1,512]{1,0:T(1,128)S(1)}, f32[1,512]{1,0:T(1,128)}, u32[]{:S(2)}) copy-start(f32[1,512]{1,0:T(1,128)} %get-tuple-element.184) | copy-start | bytes 6148
  229.6 15.5 %copy-start.39 = (f32[1,512]{1,0:T(1,128)S(1)}, f32[1,512]{1,0:T(1,128)}, u32[]{:S(2)}) copy-start(f32[1,512]{1,0:T(1,128)} %get-tuple-element.185) | copy-start | bytes 6148
  229.6 15.5 %copy-start.40 = (f32[1,512]{1,0:T(1,128)S(1)}, f32[1,512]{1,0:T(1,128)}, u32[]{:S(2)}) copy-start(f32[1,512]{1,0:T(1,128)} %get-tuple-element.186) | copy-start | bytes 6148
  229.6 15.5 %copy-start.41 = (f32[1,512]{1,0:T(1,128)S(1)}, f32[1,512]{1,0:T(1,128)}, u32[]{:S(2)}) copy-start(f32[1,512]{1,0:T(1,128)} %get-tuple-element.187) | copy-start | bytes 6148
  229.6 15.5 %copy-start.22 = (f32[2,512]{1,0:T(2,128)S(1)}, f32[2,512]{1,0:T(2,128)}, u32[]{:S(2)}) copy-start(f32[2,512]{1,0:T(2,128)} %get-tuple-element.217) | copy-start | bytes 12292
  229.6 15.5 %copy-start.21 = (f32[2,512]{1,0:T(2,128)S(1)}, f32[2,512]{1,0:T(2,128)}, u32[]{:S(2)}) copy-start(f32[2,512]{1,0:T(2,128)} %get-tuple-element.216) | copy-start | bytes 12292
  229.6 15.6 %copy-start.18 = (f32[3,512]{1,0:T(4,128)S(1)}, f32[3,512]{1,0:T(4,128)}, u32[]{:S(2)}) copy-start(f32[3,512]{1,0:T(4,128)} %slice.423) | copy-start | bytes 18436
  229.6 15.6 %copy-start.19 = (f32[3,512]{1,0:T(4,128)S(1)}, f32[3,512]{1,0:T(4,128)}, u32[]{:S(2)}) copy-start(f32[3,512]{1,0:T(4,128)} %slice.440) | copy-start | bytes 18436
  229.7 15.6 %copy-start.36 = (f32[1,512]{1,0:T(1,128)S(1)}, f32[1,512]{1,0:T(1,128)}, u32[]{:S(2)}) copy-start(f32[1,512]{1,0:T(1,128)} %slice.533) | copy-start | bytes 6148
  229.7 15.7 %copy-start.35 = (f32[1,512]{1,0:T(1,128)S(1)}, f32[1,512]{1,0:T(1,128)}, u32[]{:S(2)}) copy-start(f32[1,512]{1,0:T(1,128)} %slice.504) | copy-start | bytes 6148
  229.7 15.7 %copy-start.16 = (f32[7,512]{1,0:T(8,128)S(1)}, f32[7,512]{1,0:T(8,128)}, u32[]{:S(2)}) copy-start(f32[7,512]{1,0:T(8,128)} %slice.442) | copy-start | bytes 43012
  229.7 15.8 %copy-start.34 = (f32[1,512]{1,0:T(1,128)S(1)}, f32[1,512]{1,0:T(1,128)}, u32[]{:S(2)}) copy-start(f32[1,512]{1,0:T(1,128)} %slice.532) | copy-start | bytes 6148
  229.7 15.8 %copy-start.33 = (f32[1,512]{1,0:T(1,128)S(1)}, f32[1,512]{1,0:T(1,128)}, u32[]{:S(2)}) copy-start(f32[1,512]{1,0:T(1,128)} %slice.503) | copy-start | bytes 6148
  229.7 15.9 %copy-start.12 = (f32[15,512]{1,0:T(8,128)S(1)}, f32[15,512]{1,0:T(8,128)}, u32[]{:S(2)}) copy-start(f32[15,512]{1,0:T(8,128)} %slice.411) | copy-start | bytes 92164
  229.7 15.9 %copy-start.13 = (f32[15,512]{1,0:T(8,128)S(1)}, f32[15,512]{1,0:T(8,128)}, u32[]{:S(2)}) copy-start(f32[15,512]{1,0:T(8,128)} %slice.444) | copy-start | bytes 92164
  237.4 9.7 %copy-start.9 = (f32[31,512]{1,0:T(8,128)S(1)}, f32[31,512]{1,0:T(8,128)}, u32[]{:S(2)}) copy-start(f32[31,512]{1,0:T(8,128)} %slice.446) | copy-start | bytes 190468
  251.8 6.5 %copy-start.29 = (f32[1,512]{1,0:T(1,128)S(1)}, f32[1,512]{1,0:T(1,128)}, u32[]{:S(2)}) copy-start(f32[1,512]{1,0:T(1,128)} %slice.528) | copy-start | bytes 6148
  269.0 5.5 %copy-start.3 = (f32[512,512]{1,0:T(8,128)S(1)}, f32[512,512]{1,0:T(8,128)}, u32[]{:S(2)}) copy-start(f32[512,512]{1,0:T(8,128)} %pad.127) | copy-start | bytes 3145732
  269.0 37.6 %copy-start.27 = (f32[1,512]{1,0:T(1,128)S(1)}, f32[1,512]{1,0:T(1,128)}, u32[]{:S(2)}) copy-start(f32[1,512]{1,0:T(1,128)} %slice.527) | copy-start | bytes 6148
  301.9 38.4 %copy-start.8 = (bf16[512,256]{1,0:T(8,128)(2,1)S(1)}, bf16[512,256]{1,0:T(8,128)(2,1)}, u32[]{:S(2)}) copy-start(bf16[512,256]{1,0:T(8,128)(2,1)} %copy-done.7) | copy-start | bytes 786436
  301.9 38.4 %slice-start = ((bf16[16,768]{1,0:T(8,128)(2,1)}), bf16[16,256]{1,0:T(8,128)(2,1)S(1)}, s32[]{:S(2)}) async-start(bf16[16,768]{1,0:T(8,128)(2,1)} %copy-done.17), calls=%async_computation.8 | async-start | bytes 16384 | tf_op jit(solution)/shard_map/slice | solution.py:93
  306.6 34.5 %copy-start.14 = (f32[512]{0:T(512)S(1)}, f32[512]{0:T(512)}, u32[]{:S(2)}) copy-start(f32[512]{0:T(512)} %custom-call) | copy-start | bytes 6148
  306.6 34.5 %copy-start.15 = (f32[512]{0:T(512)S(1)}, f32[512]{0:T(512)}, u32[]{:S(2)}) copy-start(f32[512]{0:T(512)} %custom-call.1) | copy-start | bytes 6148
  306.6 34.9 %copy-start.44 = (f32[512]{0:T(512)S(1)}, f32[512]{0:T(512)}, u32[]{:S(2)}) copy-start(f32[512]{0:T(512)} %param.29) | copy-start | bytes 6148
  306.6 35.0 %copy-start.42 = (s32[512]{0:T(512)S(1)}, s32[512]{0:T(512)}, u32[]{:S(2)}) copy-start(s32[512]{0:T(512)} %add_add_fusion) | copy-start | bytes 6148
  306.6 35.0 %copy-start.46 = (s32[256]{0:T(256)S(1)}, s32[256]{0:T(256)}, u32[]{:S(2)}) copy-start(s32[256]{0:T(256)} %fusion.65) | copy-start | bytes 3076
  306.6 35.0 %copy-start.47 = (pred[256]{0:T(512)(128)(4,1)S(1)}, pred[256]{0:T(512)(128)(4,1)}, u32[]{:S(2)}) copy-start(pred[256]{0:T(512)(128)(4,1)} %get-tuple-element.200) | copy-start | bytes 772
  306.6 35.0 %copy-start.48 = (pred[256]{0:T(512)(128)(4,1)S(1)}, pred[256]{0:T(512)(128)(4,1)}, u32[]{:S(2)}) copy-start(pred[256]{0:T(512)(128)(4,1)} %get-tuple-element.201) | copy-start | bytes 772
  306.6 35.0 %copy-start.49 = (pred[256]{0:T(512)(128)(4,1)S(1)}, pred[256]{0:T(512)(128)(4,1)}, u32[]{:S(2)}) copy-start(pred[256]{0:T(512)(128)(4,1)} %get-tuple-element.202) | copy-start | bytes 772
  306.6 35.0 %copy-start.50 = (pred[256]{0:T(512)(128)(4,1)S(1)}, pred[256]{0:T(512)(128)(4,1)}, u32[]{:S(2)}) copy-start(pred[256]{0:T(512)(128)(4,1)} %get-tuple-element.203) | copy-start | bytes 772
  306.6 35.0 %copy-start.51 = (pred[256]{0:T(512)(128)(4,1)S(1)}, pred[256]{0:T(512)(128)(4,1)}, u32[]{:S(2)}) copy-start(pred[256]{0:T(512)(128)(4,1)} %get-tuple-element.204) | copy-start | bytes 772
  341.6 7.3 %copy-start.45 = (f32[256]{0:T(256)S(1)}, f32[256]{0:T(256)}, u32[]{:S(2)}) copy-start(f32[256]{0:T(256)} %param.23) | copy-start | bytes 3076
  (13 other events, 32.5 us)
Sparse Core Ops, SparseCore 0:
  8.9 13.2 all-gather.8
  24.3 41.4 all-gather.10
  68.0 47.7 all-gather.12
  117.8 38.7 all-gather.14
  158.6 47.7 all-gather.16
  208.4 47.6 all-gather.18
  362.3 9.2 reduce-scatter.1
where the time goes:
time: 385 us; the launch traced here: 381 us
  local copies, waits for them, and re-layouts  123 us (32%)
  waiting for transfers between devices  108 us (28%)
  blocking collectives  53 us (14%)
  other arithmetic  52.5 us (14%)
  matrix products  26.8 us (7%)
  between operations  14.5 us (4%)
    slice x60, local copies, waits for them, and re-layouts, shards(): lax.associative_scan(chain_pairs, (decays, drives), axis=0)  87.8 us
    all_gather x2, blocking collectives, carried_in(): everything = jax.tree.map(lambda part: lax.all_gather(part, axis), array)  53 us
    all_gather x1, waiting for transfers between devices, shards(): lax.all_gather(value_in, 'sp', axis=0, tiled=True)  47.2 us
    all_gather x1, waiting for transfers between devices, shards(): lax.all_gather(pool_in, 'sp', axis=0, tiled=True)  41.4 us
    pad x32, local copies, waits for them, and re-layouts, shards(): lax.associative_scan(chain_pairs, (decays, drives), axis=0)  24.2 us
    add x16, other arithmetic, chain_pairs(): second_pair[0] * first_pair[1] + second_pair[1]  17.6 us
    dot_general x2, matrix products, right_product(): lax.dot_general(left_rows, weight_rows, (((1,), (1,)), ((), ())), preferr...  13.1 us
    reduce_scatter x1, waiting for transfers between devices, shards(): lax.psum_scatter(right_product(pool_out, averaging_exit_matrix) + right_p...  9.43 us
  transfers between devices with their start and end apart: 8, of which 4 were waited for; matrix products, arithmetic and copies ran while one was open for 49% of the time, Pallas kernels for 0%

commit v1 on v0

--- a/solution.py
+++ b/solution.py
@@ -66,7 +66,9 @@
     gathered = (
         lax.all_gather(pool_in, "sp", axis=0, tiled=True),
         lax.all_gather(gate_in, "sp", axis=0, tiled=True),
-        lax.all_gather(value_in, "sp", axis=0, tiled=True),
+        jnp.concatenate(
+            lax.all_to_all(jnp.stack([value_in] * lax.axis_size("sp")), "sp", 0, 0), axis=0
+        ),
         lax.all_gather(out_pool, "sp", axis=0, tiled=True),
         lax.all_gather(out_rnn, "sp", axis=0, tiled=True),
     )

time: 385 us -> 354 us (0.919)
  waiting for transfers between devices: 108 us -> 66.2 us
  starting transfers between devices: 2.89 us -> 11 us
    all_gather x1 -> x0, waiting for transfers between devices: 47.2 us -> none  [shards(): lax.all_gather(value_in, 'sp', axis=0, tiled=True)]
    all_gather x1, waiting for transfers between devices: 41.4 us -> 53.6 us  [shards(): lax.all_gather(pool_in, 'sp', axis=0, tiled=True)]
    all_to_all x0 -> x1, starting transfers between devices: none -> 7.44 us  [shards(): lax.all_to_all(jnp.stack([value_in] * lax.axis_size('sp')), 'sp', 0, 0)]
    all_gather x1, waiting for transfers between devices: 6.56 us -> 0.02 us  [shards(): lax.all_gather(tokens, 'tp', axis=0, tiled=True).astype(jnp.float32)]
  transfers between devices with their start and end apart: 8 -> 8, of which waited for: 4 -> 2; matrix products, arithmetic and copies ran while one was open for 49% -> 55% of each run, Pallas kernels for 0% -> 0%
where the time goes in v1:
time: 354 us; the launch traced here: 350 us
  local copies, waits for them, and re-layouts  126 us (36%)
  waiting for transfers between devices  66.2 us (19%)
  blocking collectives  53.2 us (15%)
  other arithmetic  53 us (15%)
  matrix products  26.5 us (7%)
  between operations  14.5 us (4%)
  starting transfers between devices  11 us (3%)
    slice x60, local copies, waits for them, and re-layouts, shards(): lax.associative_scan(chain_pairs, (decays, drives), axis=0)  88 us
    all_gather x1, waiting for transfers between devices, shards(): lax.all_gather(pool_in, 'sp', axis=0, tiled=True)  53.6 us
    all_gather x2, blocking collectives, carried_in(): everything = jax.tree.map(lambda part: lax.all_gather(part, axis), array)  53.2 us
    pad x32, local copies, waits for them, and re-layouts, shards(): lax.associative_scan(chain_pairs, (decays, drives), axis=0)  24.3 us
    add x16, other arithmetic, chain_pairs(): second_pair[0] * first_pair[1] + second_pair[1]  17.8 us
    dot_general x2, matrix products, right_product(): lax.dot_general(left_rows, weight_rows, (((1,), (1,)), ((), ())), preferr...  13.1 us
    reduce_scatter x1, waiting for transfers between devices, shards(): lax.psum_scatter(right_product(pool_out, averaging_exit_matrix) + right_p...  9.4 us
    all_to_all x1, starting transfers between devices, shards(): lax.all_to_all(jnp.stack([value_in] * lax.axis_size('sp')), 'sp', 0, 0)  7.44 us
  transfers between devices with their start and end apart: 8, of which 2 were waited for; matrix products, arithmetic and copies ran while one was open for 55% of the time, Pallas kernels for 0%

profile of v1, /device:TPU:0, one launch (start us, length us, event | category | flops | bytes accessed | tf_op | source)
XLA Modules:
  0.0 350.3 jit_solution(1891000158695628767)
XLA Ops:
  9.3 2.4 stack.2
  11.8 7.4 %all-to-all-start = ((bf16[8,256,512]{2,1,0:T(8,128)(2,1)}), bf16[8,256,512]{2,1,0:T(8,128)(2,1)}, u32[]{:S(2)}, u32[]{:S(2)}) async-start(bf16[8,256,512]{2,1,0:T(8,128)(2,1)} %stack.2), calls=%async_computation | async-start | bytes 4194304 | tf_op jit(solution)/shard_map/all_to_all | solution.py:70
  25.2 2.2 fusion
  27.5 53.6 %all-gather.10.cloned.1.call-done = bf16[2048,256]{1,0:T(8,128)(2,1)} async-done(((bf16[256,256]{1,0:T(8,128)(2,1)}), bf16[2048,256]{1,0:T(8,128)(2,1)}) %all-gather.10.cloned.1.call-update) | async-done | bytes 1048592 | tf_op jit(solution)/shard_map/all_gather | solution.py:67
  81.0 2.0 convolution_convert_fusion.2
  83.7 2.9 convolution_convert_fusion.1
  87.4 3.4 collective-permute-start
  95.9 2.0 copy.30
  97.9 1.6 convolution_bitcast_fusion
  99.6 1.9 fusion.12
  101.4 2.5 copy.31
  104.0 2.5 copy.33
  106.5 4.5 %convert_multiply_fusion.5 = (f32[512,512]{1,0:T(8,128)}, f32[512,512]{1,0:T(8,128)}) fusion(f32[512,512]{1,0:T(8,128)} %copy.33, f32[512,512]{1,0:T(8,128)} %copy.32, f32[512,512]{1,0:T(8,128)} %copy.31, f32[512]{0:T(512)S(1)} %fusion.63, f32[528,512]{1,0:T(8,128)S(1)} %maximum_convert_fusion, f32[512]{0:T(512)S(1)} %bitcast.62, f32[512]{0:T(512)S(1)} %bitcast.64, ...), kind=kLoop, calls=%fused_computation.41 | loop fusion | flops 3932160 | bytes 9447424 | tf_op jit(solution)/shard_map/mul | solution.py:140
  111.0 3.8 %slice.389 = f32[256,512]{1,0:T(8,128)} slice(f32[512,512]{1,0:T(8,128)} %get-tuple-element.154), slice={[0:511:2], [0:512:1]} | slice | bytes 1048576 | tf_op jit(solution)/shard_map/slice | solution.py:141
  114.8 3.6 %slice.390 = f32[256,512]{1,0:T(8,128)} slice(f32[512,512]{1,0:T(8,128)} %get-tuple-element.154), slice={[1:512:2], [0:512:1]} | slice | bytes 1048576 | tf_op jit(solution)/shard_map/slice | solution.py:141
  118.4 2.1 slice.388
  120.5 2.1 slice.392
  122.6 2.7 multiply_add_fusion.1
  125.3 2.5 slice.395
  127.8 2.5 slice.396
  130.3 2.5 slice.394
  132.8 2.5 slice.398
  135.3 2.0 multiply_add_fusion.2
  141.9 1.9 multiply_add_fusion.3
  149.9 1.6 multiply_add_fusion.4
  194.6 1.6 slice.399
  199.0 2.5 slice.393
  201.5 2.5 slice.450
  206.6 2.1 slice.387
  208.7 3.7 %slice.452 = f32[255,512]{1,0:T(8,128)} slice(f32[512,512]{1,0:T(8,128)} %get-tuple-element.154), slice={[2:512:2], [0:512:1]} | slice | bytes 1044480 | tf_op jit(solution)/shard_map/slice | solution.py:141
  219.0 1.9 fusion.49
  223.0 4.6 %pad.127 = f32[512,512]{1,0:T(8,128)} pad(f32[256,512]{1,0:T(8,128)} %add.492, f32[]{:T(128)} %constant.117.clone.1), padding=1_0_1x0_0_0 | pad | bytes 1572868 | tf_op jit(solution)/shard_map/pad | solution.py:141
  227.6 1.7 pad_maximum_fusion.3
  229.3 2.7 pad.142
  231.9 1.7 pad.143
  233.6 2.1 add.502
  235.7 2.7 fusion.20
  239.2 4.6 %pad.126 = f32[512,512]{1,0:T(8,128)} pad(f32[256,512]{1,0:T(8,128)} %pad_maximum_fusion, f32[]{:T(128)} %constant.117.clone.1), padding=0_1_1x0_0_0 | pad | bytes 1572868 | tf_op jit(solution)/shard_map/pad | solution.py:141
  244.6 26.8 %all-gather.1 = f32[8,1,512]{2,1,0:T(1,128)S(1)} all-gather(f32[1,1,512]{2,1,0:T(1,128)S(1)} %add_bitcast_fusion), channel_id=1, replica_groups=mesh['sp'=8,'fs'=2,'tp'=2] {'sp'}, dimensions={0}, use_global_device_ids=true | all-gather | bytes 18432 | tf_op jit(solution)/shard_map/all_gather | solution.py:22
  271.4 4.6 %pad.145 = f32[512,512]{1,0:T(8,128)} pad(f32[256,512]{1,0:T(8,128)} %add.502, f32[]{:T(128)} %constant.117.clone.1), padding=1_0_1x0_0_0 | pad | bytes 1572868 | tf_op jit(solution)/shard_map/pad | solution.py:141
  276.1 1.9 pad_maximum_fusion.1
  278.0 4.6 %pad.144 = f32[512,512]{1,0:T(8,128)} pad(f32[256,512]{1,0:T(8,128)} %pad_maximum_fusion.1, f32[]{:T(128)} %constant.117.clone.1), padding=0_1_1x0_0_0 | pad | bytes 1572868 | tf_op jit(solution)/shard_map/pad | solution.py:141
  283.3 26.3 %all-gather = f32[8,1,512]{2,1,0:T(1,128)S(1)} all-gather(f32[1,1,512]{2,1,0:T(1,128)S(1)} %add_bitcast_fusion.1), channel_id=1, replica_groups=mesh['sp'=8,'fs'=2,'tp'=2] {'sp'}, dimensions={0}, use_global_device_ids=true | all-gather | bytes 18432 | tf_op jit(solution)/shard_map/all_gather | solution.py:22
  311.1 6.9 %fusion.46 = f32[2,512,128]{1,2,0:T(8,128)S(1)} fusion(bf16[2,128,128]{2,1,0:T(8,128)(2,1)S(1)} %copy-done, bf16[512,256]{1,0:T(8,128)(2,1)S(1)} %copy-done.8, s32[256]{0:T(256)S(1)} %copy-done.46, s32[512]{0:T(512)S(1)} %copy-done.42, f32[528,256]{1,0:T(8,128)} %maximum_convert_fusion.1, pred[256]{0:T(512)(128)(4,1)S(1)} %copy-done.47, ...), kind=kOutput, calls=%fused_computation.93 | convolution fusion | flops 38404096 | bytes 9250560 | tf_op jit(solution)/shard_map/tgc,gcd->tgd/dot_general | solution.py:112
  318.2 4.0 %fusion.77 = f32[512,2048]{1,0:T(8,128)} fusion(bf16[512,256]{0,1:T(8,128)(2,1)S(1)} %fusion.38, bf16[2048,256]{1,0:T(8,128)(2,1)} %all-gather.12.cloned.1.call-done), kind=kOutput, calls=%fused_computation.191 | convolution fusion | flops 536870912 | bytes 5505024 | tf_op jit(solution)/shard_map/dot_general | solution.py:42
  322.2 9.1 %convolution_add_fusion = f32[512,2048]{1,0:T(8,128)} fusion(f32[512,2048]{1,0:T(8,128)} %fusion.77, bf16[2048,512]{1,0:T(8,128)(2,1)} %all-gather.16.cloned.1.call-done, bf16[2048,512]{1,0:T(8,128)(2,1)} %all-gather.14.cloned.1.call-done, f32[512,512]{1,0:T(8,128)} %pad.144, f32[512,512]{1,0:T(8,128)} %pad.145, f32[512,512]{1,0:T(8,128)} %pad.126, ...), kind=kOutput, calls=%fused_computation.9 | convolution fusion | flops 2156920832 | bytes 18886656 | tf_op jit(solution)/shard_map/dot_general | solution.py:42
  331.3 9.4 %reduce-scatter.2.cloned.1.call-done = f32[256,2048]{1,0:T(8,128)} async-done(((f32[512,2048]{1,0:T(8,128)}), f32[256,2048]{1,0:T(8,128)}) %reduce-scatter.2.cloned.1.call-update) | async-done | bytes 2097168 | tf_op jit(solution)/shard_map/reduce_scatter | solution.py:151
  340.7 2.7 convert_element_type.63
  (282 shorter events, 86.4 us)
Async XLA Ops:
  6.5 304.4 %copy-start = (bf16[2,128,128]{2,1,0:T(8,128)(2,1)S(1)}, bf16[2,128,128]{2,1,0:T(8,128)(2,1)}, u32[]{:S(2)}) copy-start(bf16[2,128,128]{2,1,0:T(8,128)(2,1)} %param.22) | copy-start | bytes 196612
  6.5 18.7 %all-gather.8.cloned.1.call-start = ((), (), s32[]{:S(2)}) async-start(), calls=%async_computation.2 | async-start | bytes 3145728 | tf_op jit(solution)/shard_map/all_gather | solution.py:78
  7.3 73.8 %all-gather.10.cloned.1.call-start = ((), (), s32[]{:S(2)}) async-start(), calls=%async_computation.3 | async-start | bytes 1179648 | tf_op jit(solution)/shard_map/all_gather | solution.py:67
  8.0 310.2 %all-gather.12.cloned.1.call-start = ((), (), s32[]{:S(2)}) async-start(), calls=%async_computation.4 | async-start | bytes 1179648 | tf_op jit(solution)/shard_map/all_gather | solution.py:72
  8.7 313.4 %all-gather.14.cloned.1.call-start = ((), (), s32[]{:S(2)}) async-start(), calls=%async_computation.5 | async-start | bytes 2359296 | tf_op jit(solution)/shard_map/all_gather | solution.py:68
  11.8 13.4 %copy-start.43 = (f32[512]{0:T(512)S(1)}, f32[512]{0:T(512)}, u32[]{:S(2)}) copy-start(f32[512]{0:T(512)} %param.27) | copy-start | bytes 6148
  11.8 13.4 %copy-start.37 = (f32[4,512]{1,0:T(4,128)S(1)}, f32[4,512]{1,0:T(4,128)}, u32[]{:S(2)}) copy-start(f32[4,512]{1,0:T(4,128)} %param.24) | copy-start | bytes 24580
  11.8 72.0 %all-to-all-start = ((bf16[8,256,512]{2,1,0:T(8,128)(2,1)}), bf16[8,256,512]{2,1,0:T(8,128)(2,1)}, u32[]{:S(2)}, u32[]{:S(2)}) async-start(bf16[8,256,512]{2,1,0:T(8,128)(2,1)} %stack.2), calls=%async_computation | async-start | bytes 4194304 | tf_op jit(solution)/shard_map/all_to_all | solution.py:70
  19.2 61.8 %copy-start.23 = (f32[2048]{0:T(1024)S(1)}, f32[2048]{0:T(1024)}, u32[]{:S(2)}) copy-start(f32[2048]{0:T(1024)} %param.18) | copy-start | bytes 24580
  19.2 303.0 %all-gather.16.cloned.1.call-start = ((), (), s32[]{:S(2)}) async-start(), calls=%async_computation.6 | async-start | bytes 2359296 | tf_op jit(solution)/shard_map/all_gather | solution.py:73
  19.8 320.9 %reduce-scatter.2.cloned.1.call-start = ((), (), s32[]{:S(2)}) async-start(), calls=%async_computation.7 | async-start | bytes 6291456 | tf_op jit(solution)/shard_map/reduce_scatter | solution.py:151
  25.2 55.8 %copy-start.1 = (bf16[512,2048]{1,0:T(8,128)(2,1)S(1)}, bf16[512,2048]{1,0:T(8,128)(2,1)}, u32[]{:S(2)}) copy-start(bf16[512,2048]{1,0:T(8,128)(2,1)} %all-gather.8.cloned.1.call-done) | copy-start | bytes 6291460
  27.5 56.3 %copy-start.25 = (f32[512]{0:T(512)}, f32[512]{0:T(512)S(1)}, u32[]{:S(2)}) copy-start(f32[512]{0:T(512)S(1)} %add_rsqrt_fusion) | copy-start | bytes 6148
  83.7 7.6 %copy-start.20 = (f32[8,512]{1,0:T(8,128)S(1)}, f32[8,512]{1,0:T(8,128)}, u32[]{:S(2)}) copy-start(f32[8,512]{1,0:T(8,128)} %param.28) | copy-start | bytes 49156
  87.4 5.4 %collective-permute-start = (bf16[16,768]{1,0:T(8,128)(2,1)S(1)}, bf16[16,768]{1,0:T(8,128)(2,1)S(1)}, u32[]{:S(2)}, u32[]{:S(2)}) collective-permute-start(bf16[16,768]{1,0:T(8,128)(2,1)S(1)} %pad_maximum_fusion.10), channel_id=1, source_target_pairs={{0,4},{4,8},{8,12},{12,16},{16,20},{20,24},{24,28},{1,5},{5,9},{9,... | collective-permute-start | bytes 73736 | tf_op jit(solution)/shard_map/ppermute | solution.py:17
  111.0 7.4 %copy-start.2 = (f32[512,512]{1,0:T(8,128)S(1)}, f32[512,512]{1,0:T(8,128)}, u32[]{:S(2)}) copy-start(f32[512,512]{1,0:T(8,128)} %get-tuple-element.155) | copy-start | bytes 3145732
  198.8 15.4 %copy-start.38 = (f32[1,512]{1,0:T(1,128)S(1)}, f32[1,512]{1,0:T(1,128)}, u32[]{:S(2)}) copy-start(f32[1,512]{1,0:T(1,128)} %get-tuple-element.184) | copy-start | bytes 6148
  198.8 15.4 %copy-start.39 = (f32[1,512]{1,0:T(1,128)S(1)}, f32[1,512]{1,0:T(1,128)}, u32[]{:S(2)}) copy-start(f32[1,512]{1,0:T(1,128)} %get-tuple-element.185) | copy-start | bytes 6148
  198.8 15.4 %copy-start.40 = (f32[1,512]{1,0:T(1,128)S(1)}, f32[1,512]{1,0:T(1,128)}, u32[]{:S(2)}) copy-start(f32[1,512]{1,0:T(1,128)} %get-tuple-element.186) | copy-start | bytes 6148
  198.8 15.4 %copy-start.41 = (f32[1,512]{1,0:T(1,128)S(1)}, f32[1,512]{1,0:T(1,128)}, u32[]{:S(2)}) copy-start(f32[1,512]{1,0:T(1,128)} %get-tuple-element.187) | copy-start | bytes 6148
  198.8 15.5 %copy-start.22 = (f32[2,512]{1,0:T(2,128)S(1)}, f32[2,512]{1,0:T(2,128)}, u32[]{:S(2)}) copy-start(f32[2,512]{1,0:T(2,128)} %get-tuple-element.217) | copy-start | bytes 12292
  198.9 15.5 %copy-start.21 = (f32[2,512]{1,0:T(2,128)S(1)}, f32[2,512]{1,0:T(2,128)}, u32[]{:S(2)}) copy-start(f32[2,512]{1,0:T(2,128)} %get-tuple-element.216) | copy-start | bytes 12292
  198.9 15.5 %copy-start.18 = (f32[3,512]{1,0:T(4,128)S(1)}, f32[3,512]{1,0:T(4,128)}, u32[]{:S(2)}) copy-start(f32[3,512]{1,0:T(4,128)} %slice.423) | copy-start | bytes 18436
  198.9 15.5 %copy-start.19 = (f32[3,512]{1,0:T(4,128)S(1)}, f32[3,512]{1,0:T(4,128)}, u32[]{:S(2)}) copy-start(f32[3,512]{1,0:T(4,128)} %slice.440) | copy-start | bytes 18436
  198.9 15.5 %copy-start.36 = (f32[1,512]{1,0:T(1,128)S(1)}, f32[1,512]{1,0:T(1,128)}, u32[]{:S(2)}) copy-start(f32[1,512]{1,0:T(1,128)} %slice.533) | copy-start | bytes 6148
  198.9 15.6 %copy-start.35 = (f32[1,512]{1,0:T(1,128)S(1)}, f32[1,512]{1,0:T(1,128)}, u32[]{:S(2)}) copy-start(f32[1,512]{1,0:T(1,128)} %slice.504) | copy-start | bytes 6148
  198.9 15.7 %copy-start.16 = (f32[7,512]{1,0:T(8,128)S(1)}, f32[7,512]{1,0:T(8,128)}, u32[]{:S(2)}) copy-start(f32[7,512]{1,0:T(8,128)} %slice.442) | copy-start | bytes 43012
  198.9 15.7 %copy-start.34 = (f32[1,512]{1,0:T(1,128)S(1)}, f32[1,512]{1,0:T(1,128)}, u32[]{:S(2)}) copy-start(f32[1,512]{1,0:T(1,128)} %slice.532) | copy-start | bytes 6148
  198.9 15.8 %copy-start.33 = (f32[1,512]{1,0:T(1,128)S(1)}, f32[1,512]{1,0:T(1,128)}, u32[]{:S(2)}) copy-start(f32[1,512]{1,0:T(1,128)} %slice.503) | copy-start | bytes 6148
  198.9 15.8 %copy-start.12 = (f32[15,512]{1,0:T(8,128)S(1)}, f32[15,512]{1,0:T(8,128)}, u32[]{:S(2)}) copy-start(f32[15,512]{1,0:T(8,128)} %slice.411) | copy-start | bytes 92164
  198.9 15.8 %copy-start.13 = (f32[15,512]{1,0:T(8,128)S(1)}, f32[15,512]{1,0:T(8,128)}, u32[]{:S(2)}) copy-start(f32[15,512]{1,0:T(8,128)} %slice.444) | copy-start | bytes 92164
  206.6 9.7 %copy-start.9 = (f32[31,512]{1,0:T(8,128)S(1)}, f32[31,512]{1,0:T(8,128)}, u32[]{:S(2)}) copy-start(f32[31,512]{1,0:T(8,128)} %slice.446) | copy-start | bytes 190468
  221.0 6.6 %copy-start.29 = (f32[1,512]{1,0:T(1,128)S(1)}, f32[1,512]{1,0:T(1,128)}, u32[]{:S(2)}) copy-start(f32[1,512]{1,0:T(1,128)} %slice.528) | copy-start | bytes 6148
  238.4 5.5 %copy-start.3 = (f32[512,512]{1,0:T(8,128)S(1)}, f32[512,512]{1,0:T(8,128)}, u32[]{:S(2)}) copy-start(f32[512,512]{1,0:T(8,128)} %pad.127) | copy-start | bytes 3145732
  238.4 37.7 %copy-start.27 = (f32[1,512]{1,0:T(1,128)S(1)}, f32[1,512]{1,0:T(1,128)}, u32[]{:S(2)}) copy-start(f32[1,512]{1,0:T(1,128)} %slice.527) | copy-start | bytes 6148
  271.4 38.2 %copy-start.8 = (bf16[512,256]{1,0:T(8,128)(2,1)S(1)}, bf16[512,256]{1,0:T(8,128)(2,1)}, u32[]{:S(2)}) copy-start(bf16[512,256]{1,0:T(8,128)(2,1)} %copy-done.7) | copy-start | bytes 786436
  271.4 38.2 %slice-start = ((bf16[16,768]{1,0:T(8,128)(2,1)}), bf16[16,256]{1,0:T(8,128)(2,1)S(1)}, s32[]{:S(2)}) async-start(bf16[16,768]{1,0:T(8,128)(2,1)} %copy-done.17), calls=%async_computation.8 | async-start | bytes 16384 | tf_op jit(solution)/shard_map/slice | solution.py:95
  276.0 34.5 %copy-start.14 = (f32[512]{0:T(512)S(1)}, f32[512]{0:T(512)}, u32[]{:S(2)}) copy-start(f32[512]{0:T(512)} %custom-call) | copy-start | bytes 6148
  276.0 34.5 %copy-start.15 = (f32[512]{0:T(512)S(1)}, f32[512]{0:T(512)}, u32[]{:S(2)}) copy-start(f32[512]{0:T(512)} %custom-call.1) | copy-start | bytes 6148
  276.0 34.9 %copy-start.44 = (f32[512]{0:T(512)S(1)}, f32[512]{0:T(512)}, u32[]{:S(2)}) copy-start(f32[512]{0:T(512)} %param.29) | copy-start | bytes 6148
  276.0 35.0 %copy-start.42 = (s32[512]{0:T(512)S(1)}, s32[512]{0:T(512)}, u32[]{:S(2)}) copy-start(s32[512]{0:T(512)} %add_add_fusion) | copy-start | bytes 6148
  276.0 35.0 %copy-start.46 = (s32[256]{0:T(256)S(1)}, s32[256]{0:T(256)}, u32[]{:S(2)}) copy-start(s32[256]{0:T(256)} %fusion.65) | copy-start | bytes 3076
  276.0 35.0 %copy-start.47 = (pred[256]{0:T(512)(128)(4,1)S(1)}, pred[256]{0:T(512)(128)(4,1)}, u32[]{:S(2)}) copy-start(pred[256]{0:T(512)(128)(4,1)} %get-tuple-element.200) | copy-start | bytes 772
  276.0 35.0 %copy-start.48 = (pred[256]{0:T(512)(128)(4,1)S(1)}, pred[256]{0:T(512)(128)(4,1)}, u32[]{:S(2)}) copy-start(pred[256]{0:T(512)(128)(4,1)} %get-tuple-element.201) | copy-start | bytes 772
  276.1 35.0 %copy-start.49 = (pred[256]{0:T(512)(128)(4,1)S(1)}, pred[256]{0:T(512)(128)(4,1)}, u32[]{:S(2)}) copy-start(pred[256]{0:T(512)(128)(4,1)} %get-tuple-element.202) | copy-start | bytes 772
  276.1 35.0 %copy-start.50 = (pred[256]{0:T(512)(128)(4,1)S(1)}, pred[256]{0:T(512)(128)(4,1)}, u32[]{:S(2)}) copy-start(pred[256]{0:T(512)(128)(4,1)} %get-tuple-element.203) | copy-start | bytes 772
  276.1 35.0 %copy-start.51 = (pred[256]{0:T(512)(128)(4,1)S(1)}, pred[256]{0:T(512)(128)(4,1)}, u32[]{:S(2)}) copy-start(pred[256]{0:T(512)(128)(4,1)} %get-tuple-element.204) | copy-start | bytes 772
  311.1 7.0 %copy-start.45 = (f32[256]{0:T(256)S(1)}, f32[256]{0:T(256)}, u32[]{:S(2)}) copy-start(f32[256]{0:T(256)} %param.23) | copy-start | bytes 3076
  (13 other events, 32.5 us)
Sparse Core Ops, SparseCore 0:
  8.9 13.2 all-gather.7
  24.3 56.6 all-gather.9
  83.2 39.7 all-gather.11
  124.9 47.7 all-gather.13
  174.7 47.6 all-gather.15
  331.5 9.2 reduce-scatter.1
